TPU v7x, 512 devices: a whole 4x4x16 slice. The times are simulated.
512 devices in a mesh: sp: 64 (over z, y), tp: 8 (over x, core).
Axes of the slice: x: 4, y: 4, z: 16, core: 2. Of those that a mesh axis runs over, the one named last changes fastest.
Arguments:
- residual: bfloat16 [8192, 2048], P('sp'), may hold values from -6 to 6
- query_nope: bfloat16 [8192, 8, 128], P('sp', 'tp'), may hold values from -6 to 6
- query_rope: bfloat16 [8192, 8, 64], P('sp', 'tp'), may hold values from -64 to 64
- latent: bfloat16 [8192, 256], P('sp'), may hold values from -6 to 6
- rope_key: bfloat16 [8192, 64], P('sp'), may hold values from -64 to 64
- kv_gain: bfloat16 [256], replicated, may hold values from 0.099609375 to 1.8984375
- key_up: bfloat16 [256, 8, 128], replicated, may hold values from -0.375 to 0.375
- value_up: bfloat16 [256, 8, 128], replicated, may hold values from -0.375 to 0.375
- out_weight: bfloat16 [1024, 2048], P('tp'), may hold values from -0.1875 to 0.1875
- post_gain: bfloat16 [2048], replicated, may hold values from 0.099609375 to 1.8984375
- pre_gain: bfloat16 [2048], replicated, may hold values from 0.099609375 to 1.8984375
- ffn_gain: bfloat16 [2048], replicated, may hold values from 0.099609375 to 1.8984375
- up_value: bfloat16 [2048, 5632], P('sp', 'tp'), may hold values from -0.125 to 0.125
- up_gate: bfloat16 [2048, 5632], P('sp', 'tp'), may hold values from -0.125 to 0.125
- conv_value: bfloat16 [3, 5632], replicated, may hold values from -3.5 to 3.5
- conv_gate: bfloat16 [3, 5632], replicated, may hold values from -3.5 to 3.5
- down_weight: bfloat16 [5632, 2048], P('tp', 'sp'), may hold values from -0.078125 to 0.078125
Outputs:
- layer_out: bfloat16 [8192, 2048], P(('sp', 'tp'))
All inputs are finite; a program needn't handle non-finite values.
Results may differ from a plain program's by a relative error of at most 0.02.
Values may be sent and summed in bfloat16 or wider, within the bound.
A program may use at most 128 MiB of HBM per device.

v0:
```python
import jax
import jax.numpy as jnp
from jax import lax
from jax.sharding import Mesh
from jax.sharding import PartitionSpec as P

GRID = 64
SP = ("sp_0", "sp_1")
SP_TP = ("sp_0", "sp_1", "tp")
epsilon = 1e-06
rope_base = 10000.0


def side_by_side(arrays, axis, dim, along):
    both = jnp.concatenate(arrays, axis=along)
    whole, at, outs = (lax.all_gather(both, axis, axis=dim, tiled=True), 0, [])
    for a in arrays:
        outs.append(lax.slice_in_dim(whole, at, at + a.shape[along], axis=along))
        at += a.shape[along]
    return tuple(outs)


def sent_to_all(x, axis):
    size = lax.axis_size(axis)
    return lax.all_to_all(jnp.broadcast_to(x[None], (size, *x.shape)), axis, 0, 0, tiled=True)


def taken_together(x, axis):
    return sent_to_all(x, axis).astype(jnp.float32).sum(axis=0)


def joined_along(pieces, dim):
    pieces = jnp.moveaxis(pieces, 0, dim)
    shape = pieces.shape
    return pieces.reshape(*shape[:dim], shape[dim] * shape[dim + 1], *shape[dim + 2 :])


def stacked_from(x, axes, order):
    pieces = x[None]
    for k in order:
        pieces = lax.all_gather(pieces, axes[k], axis=0, tiled=True)
    current = [lax.axis_size(axes[k]) for k in reversed(order)]
    pieces = pieces.reshape(*current, *x.shape)
    turned = sorted(range(len(order)), key=lambda place: order[len(order) - 1 - place])
    return pieces.transpose(*turned, *range(len(order), pieces.ndim)).reshape(-1, *x.shape)


def gathered_by_axis(x, axes, order, dim):
    return joined_along(stacked_from(x, axes, order), dim)


def extended(x, sides, width):
    for axis, dim in sides:
        size, length = (lax.axis_size(axis), x.shape[dim])
        up = [(i, (i + 1) % size) for i in range(size - 1)]
        down = [(j, i) for i, j in up]
        last = lax.slice_in_dim(x, length - width, length, axis=dim)
        initial = lax.slice_in_dim(x, 0, width, axis=dim)
        before = lax.ppermute(last, axis, up)
        after = lax.ppermute(initial, axis, down)
        x = jnp.concatenate([before, x, after], axis=dim)
    return x


def whole_of(x, axes, dim):
    for axis in reversed(axes):
        x = lax.all_gather(x, axis, axis=dim, tiled=True)
    return x


def split_up(x, dim, size):
    shape = x.shape
    pieces = x.reshape(*shape[:dim], size, shape[dim] // size, *shape[dim + 1 :])
    return jnp.moveaxis(pieces, dim, 0)


def sum_at_owner(x, axis, dim):
    size = lax.axis_size(axis)
    pieces = lax.all_to_all(split_up(x, dim, size), axis, 0, 0, tiled=True)
    return jnp.sum(pieces.astype(jnp.float32), axis=0)


def rms_norm(values, gain):
    return (
        values
        * lax.rsqrt(jnp.mean(values * values, axis=-1, keepdims=True) + epsilon)
        * gain.astype(jnp.float32)
    )


def widened(values):
    return lax.optimization_barrier(values.astype(jnp.bfloat16)).astype(jnp.float32)


def rotate(values, positions):
    pair_count = values.shape[-1] // 4
    frequency = rope_base ** (-jnp.arange(pair_count, dtype=jnp.float32) / pair_count)
    grid_rows = (positions // GRID).astype(jnp.float32)
    grid_cols = (positions % GRID).astype(jnp.float32)
    angles = jnp.stack([grid_rows, grid_cols], axis=-1)[:, :, None] * frequency
    table_shape = (angles.shape[0],) + (1,) * (values.ndim - 2) + angles.shape[1:]
    cosine = jnp.cos(angles).reshape(table_shape)
    sine = jnp.sin(angles).reshape(table_shape)
    halves = values.reshape(values.shape[:-1] + (2, 2, pair_count))
    leading = halves[..., 0, :]
    trailing = halves[..., 1, :]
    turned = jnp.stack(
        [leading * cosine - trailing * sine, trailing * cosine + leading * sine], axis=-2
    )
    return turned.reshape(values.shape)


def body(
    residual,
    query_nope,
    query_rope,
    latent,
    rope_key,
    kv_gain,
    key_up,
    value_up,
    out_weight,
    post_gain,
    pre_gain,
    ffn_gain,
    up_value,
    up_gate,
    conv_value,
    conv_gate,
    down_weight,
):
    tok_rows = residual.shape[0]
    heads_dev = query_nope.shape[1]
    value_width = value_up.shape[2]
    tp_index = lax.axis_index("tp")
    positions = lax.axis_index(SP) * tok_rows + jnp.arange(tok_rows, dtype=jnp.int32)
    score_scale = (query_nope.shape[2] + query_rope.shape[2]) ** (-0.5)
    normed = rms_norm(latent.astype(jnp.float32), kv_gain).astype(jnp.bfloat16)
    key_turn = rotate(rope_key.astype(jnp.float32), positions).astype(jnp.bfloat16)
    query_turn = rotate(query_rope.astype(jnp.float32), positions).astype(jnp.bfloat16)
    key_local = lax.dynamic_slice_in_dim(key_up, tp_index * heads_dev, heads_dev, 1)
    value_local = lax.dynamic_slice_in_dim(value_up, tp_index * heads_dev, heads_dev, 1)
    pieces = side_by_side((normed, key_turn), SP, 0, 1)
    keys_nope = jnp.einsum(
        "nc,chd->nhd", pieces[0], key_local, preferred_element_type=jnp.float32
    ).astype(jnp.bfloat16)
    values_part = jnp.einsum(
        "nc,chd->nhd", pieces[0], value_local, preferred_element_type=jnp.float32
    ).astype(jnp.bfloat16)
    row_max = jnp.full((heads_dev, tok_rows), -1e30, jnp.float32)
    scores = (
        jnp.einsum("qhd,khd->hqk", query_nope, keys_nope, preferred_element_type=jnp.float32)
        + jnp.einsum("qhd,kd->hqk", query_turn, pieces[1], preferred_element_type=jnp.float32)
    ) * score_scale
    new_max = jnp.maximum(row_max, jnp.max(scores, axis=-1))
    weights = jnp.exp(scores - new_max[:, :, None])
    totals = jnp.sum(weights, axis=-1)
    weighted = jnp.einsum(
        "hqk,khd->hqd",
        weights.astype(jnp.bfloat16),
        values_part,
        preferred_element_type=jnp.float32,
    )
    attended = (weighted / totals[:, :, None]).astype(jnp.bfloat16)
    attended = jnp.transpose(attended, (1, 0, 2)).reshape(tok_rows, heads_dev * value_width)
    row_share = tok_rows // lax.axis_size("tp")
    summed = taken_together(
        jnp.dot(attended, out_weight, preferred_element_type=jnp.float32).astype(jnp.bfloat16), "tp"
    ).astype(jnp.float32)
    stream_all = widened(residual.astype(jnp.float32) + rms_norm(widened(summed), post_gain))
    inputs = rms_norm(stream_all, pre_gain).astype(jnp.bfloat16)
    stream_wide = lax.dynamic_slice_in_dim(stream_all, tp_index * row_share, row_share, 0)
    ff_dev = up_value.shape[1]
    up_joined = jnp.concatenate([up_value, up_gate], axis=1)
    up_whole = gathered_by_axis(up_joined, SP, (0, 1), 0)
    up_pair = jnp.dot(inputs, up_whole, preferred_element_type=jnp.float32).astype(jnp.bfloat16)
    padded = extended(up_pair, ((SP, 0),), 1).astype(jnp.float32)
    channel_start = tp_index * ff_dev
    conv_taps = jnp.concatenate(
        [
            lax.dynamic_slice_in_dim(conv_value, channel_start, ff_dev, 1),
            lax.dynamic_slice_in_dim(conv_gate, channel_start, ff_dev, 1),
        ],
        axis=1,
    ).astype(jnp.float32)
    mixed_conv = (
        padded[:-2] * conv_taps[0] + padded[1:-1] * conv_taps[1] + padded[2:] * conv_taps[2]
    )
    hidden = (jax.nn.silu(mixed_conv[:, ff_dev:]) * mixed_conv[:, :ff_dev]).astype(jnp.bfloat16)
    down_whole = whole_of(down_weight, SP, 1)
    down_terms = jnp.dot(hidden, down_whole, preferred_element_type=jnp.float32)
    reduced = sum_at_owner(down_terms.astype(jnp.bfloat16), "tp", 0)
    return (stream_wide + rms_norm(widened(reduced), ffn_gain)).astype(jnp.bfloat16)


def solution(mesh):
    torus = Mesh(mesh.devices.reshape(16, 4, mesh.shape["tp"]), ("sp_0", "sp_1", "tp"))
    return jax.shard_map(
        body,
        mesh=torus,
        in_specs=(
            P(SP, None),
            P(SP, "tp", None),
            P(SP, "tp", None),
            P(SP, None),
            P(SP, None),
            P(),
            P(),
            P(),
            P("tp", None),
            P(),
            P(),
            P(),
            P(SP, "tp"),
            P(SP, "tp"),
            P(),
            P(),
            P("tp", SP),
        ),
        out_specs=P(SP_TP, None),
        check_vma=False,
    )
```

profile of v0, /device:TPU:1, one launch (start us, length us, event | category | flops | bytes accessed | tf_op | source)
XLA Modules:
  0.0 408.5 jit_solution(6371514957831806207)
XLA Ops:
  6.5 1.6 pad_maximum_fusion.1
  9.9 0.9 fusion.37
  12.6 64.1 %all-gather.12.cloned.1.call-done = bf16[512,1408]{1,0:T(8,128)(2,1)} async-done(((bf16[32,1408]{1,0:T(8,128)(2,1)}), bf16[512,1408]{1,0:T(8,128)(2,1)}) %all-gather.12.cloned.1.call-update) | async-done | bytes 1441808 | tf_op jit(solution)/shard_map/all_gather | solution.py:41
  77.6 1.5 constant_dynamic-slice_fusion.2
  79.1 149.7 %all-gather.6.cloned.1.call-done = bf16[8192,320]{1,0:T(8,128)(2,1)} async-done(((bf16[128,320]{1,0:T(8,128)(2,1)}), bf16[8192,320]{1,0:T(8,128)(2,1)}) %all-gather.6.cloned.1.call-update) | async-done | bytes 5242896 | tf_op jit(solution)/shard_map/all_gather | solution.py:16
  228.8 4.2 %convolution_bitcast_fusion = f32[1,128,8192]{1,2,0:T(8,128)} fusion(bf16[128,64]{0,1:T(8,128)(2,1)S(1)} %bitcast.54, bf16[8192,320]{1,0:T(8,128)(2,1)} %all-gather.6.cloned.1.call-done), kind=kOutput, calls=%fused_computation | convolution fusion | flops 134217728 | bytes 6307840 | tf_op jit(solution)/shard_map/qhd,kd->hqk/dot_general | solution.py:153
  233.0 7.6 %fusion.67 = (f32[128]{0:T(128)S(1)}, f32[1,128,8192]{1,2,0:T(8,128)}) fusion(f32[1,128,8192]{1,2,0:T(8,128)} %convolution_bitcast_fusion, bf16[128,1,128]{2,0,1:T(8,128)(2,1)S(1)} %copy-done.3, bf16[8192,320]{1,0:T(8,128)(2,1)} %all-gather.6.cloned.1.call-done, bf16[256,1,128]{2,1,0:T(2,128)(2,1)S(1)} %get-tuple-element.19), kind=kOutput, calls=%fused_computation.104 | convolution fusion | flops 809500544 | bytes 12681728 | tf_op jit(solution)/shard_map/qhd,khd->hqk/dot_general | solution.py:152
  240.6 3.3 fusion.2
  243.8 5.7 %fusion.20 = bf16[128,128]{1,0:T(8,128)(2,1)S(1)} fusion(bf16[8192,320]{1,0:T(8,128)(2,1)} %all-gather.6.cloned.1.call-done, f32[1,128,8192]{1,2,0:T(8,128)} %get-tuple-element.15, f32[128]{0:T(128)S(1)} %broadcast_maximum_fusion, bf16[256,1,128]{2,1,0:T(2,128)(2,1)S(1)} %get-tuple-element.18, f32[128]{0:T(128)S(1)} %fusion.2), kind=kOutput, calls=%fused_computation.21 | convolution fusion | flops 808484864 | bytes 8487936 | tf_op jit(solution)/shard_map/hqk,khd->hqd/dot_general | solution.py:158
  249.9 2.5 broadcast_in_dim.7
  252.4 14.1 %all-to-all-start = ((bf16[8,128,2048]{2,1,0:T(8,128)(2,1)}), bf16[8,128,2048]{2,1,0:T(8,128)(2,1)}, u32[]{:S(2)}, u32[]{:S(2)}) async-start(bf16[8,128,2048]{2,1,0:T(8,128)(2,1)} %broadcast_in_dim.7), calls=%async_computation | async-start | bytes 8388608 | tf_op jit(solution)/shard_map/all_to_all | solution.py:25
  266.5 12.0 %all_gather.18 = bf16[704,128]{0,1:T(8,128)(2,1)} all-gather(bf16[704,32]{0,1:T(8,128)(2,1)S(1)} %copy-done.2), channel_id=1, replica_groups=mesh['sp_0'=16,'sp_1'=4,'tp'=8] {'sp_1'}, dimensions={1}, use_global_device_ids=true | all-gather | bytes 225280 | tf_op jit(solution)/shard_map/all_gather | solution.py:67
  279.3 25.3 %all-gather.8.cloned.1.call-done = bf16[64,32,1408]{2,1,0:T(8,128)(2,1)} async-done(((bf16[16,32,1408]{2,1,0:T(8,128)(2,1)}), bf16[64,32,1408]{2,1,0:T(8,128)(2,1)}) %all-gather.8.cloned.1.call-update) | async-done | bytes 5767184 | tf_op jit(solution)/shard_map/all_gather | solution.py:41
  304.7 5.8 %copy.33 = bf16[16,4,32,1408]{3,2,1,0:T(8,128)(2,1)} copy(bf16[16,4,32,1408]{3,2,0,1:T(8,128)(2,1)} %bitcast.52) | data formatting | bytes 11534336 | tf_op jit(solution)/shard_map/transpose | solution.py:45
  310.5 4.7 %all-to-all-done = bf16[8,128,2048]{2,1,0:T(8,128)(2,1)} async-done(((bf16[8,128,2048]{2,1,0:T(8,128)(2,1)}), bf16[8,128,2048]{2,1,0:T(8,128)(2,1)}, u32[]{:S(2)}, u32[]{:S(2)}) %all-to-all-start) | async-done | bytes 4194336 | tf_op jit(solution)/shard_map/all_to_all | solution.py:25
  315.3 3.0 reduce_sum.71
  318.9 3.7 convolution_convert_fusion.4
  322.6 2.5 collective-permute-start
  325.1 1.3 collective-permute-start.1
  326.5 3.3 collective-permute-done.1
  330.2 43.6 %all-gather.10.cloned.1.call-done = bf16[704,2048]{0,1:T(8,128)(2,1)} async-done(((bf16[704,128]{0,1:T(8,128)(2,1)}), bf16[704,2048]{0,1:T(8,128)(2,1)}) %all-gather.10.cloned.1.call-update) | async-done | bytes 2883600 | tf_op jit(solution)/shard_map/all_gather | solution.py:67
  373.8 3.9 convolution_convert_fusion.2
  377.6 14.0 %all-to-all-start.1 = ((bf16[8,16,2048]{2,1,0:T(8,128)(2,1)}), bf16[8,16,2048]{2,1,0:T(8,128)(2,1)S(1)}, u32[]{:S(2)}, u32[]{:S(2)}) async-start(bf16[8,16,2048]{2,1,0:T(8,128)(2,1)} %bitcast.18), calls=%async_computation.1 | async-start | bytes 1048576 | tf_op jit(solution)/shard_map/all_to_all | solution.py:79
  391.8 9.2 %all-to-all-done.1 = bf16[8,16,2048]{2,1,0:T(8,128)(2,1)S(1)} async-done(((bf16[8,16,2048]{2,1,0:T(8,128)(2,1)}), bf16[8,16,2048]{2,1,0:T(8,128)(2,1)S(1)}, u32[]{:S(2)}, u32[]{:S(2)}) %all-to-all-start.1) | async-done | bytes 524320 | tf_op jit(solution)/shard_map/all_to_all | solution.py:79
  (57 shorter events, 7.6 us)
Async XLA Ops:
  6.5 243.0 %copy-start = (bf16[128,2048]{1,0:T(8,128)(2,1)S(1)}, bf16[128,2048]{1,0:T(8,128)(2,1)}, u32[]{:S(2)}) copy-start(bf16[128,2048]{1,0:T(8,128)(2,1)} %param.25) | copy-start | bytes 1572868
  6.5 70.1 %all-gather.12.cloned.1.call-start = ((), (), s32[]{:S(2)}) async-start(), calls=%async_computation.5 | async-start | bytes 1531904 | tf_op jit(solution)/shard_map/all_gather | solution.py:41
  8.2 220.6 %all-gather.6.cloned.1.call-start = ((), (), s32[]{:S(2)}) async-start(), calls=%async_computation.2 | async-start | bytes 6389760 | tf_op jit(solution)/shard_map/all_gather | solution.py:16
  12.5 292.2 %all-gather.8.cloned.1.call-start = ((), (), s32[]{:S(2)}) async-start(), calls=%async_computation.3 | async-start | bytes 7208960 | tf_op jit(solution)/shard_map/all_gather | solution.py:41
  77.6 155.4 %copy-start.3 = (bf16[128,1,128]{2,0,1:T(8,128)(2,1)S(1)}, bf16[128,1,128]{2,0,1:T(8,128)(2,1)}, u32[]{:S(2)}) copy-start(bf16[128,1,128]{2,0,1:T(8,128)(2,1)} %param.18) | copy-start | bytes 98308
  252.4 14.1 %copy-start.2 = (bf16[704,32]{0,1:T(8,128)(2,1)S(1)}, bf16[704,32]{0,1:T(8,128)(2,1)}, u32[]{:S(2)}) copy-start(bf16[704,32]{0,1:T(8,128)(2,1)} %param.33) | copy-start | bytes 135172
  252.4 26.1 %copy-start.4 = (bf16[2048]{0:T(1024)(128)(2,1)S(1)}, bf16[2048]{0:T(1024)(128)(2,1)}, u32[]{:S(2)}) copy-start(bf16[2048]{0:T(1024)(128)(2,1)} %param.26) | copy-start | bytes 12292
  252.4 26.1 %copy-start.5 = (bf16[2048]{0:T(1024)(128)(2,1)S(1)}, bf16[2048]{0:T(1024)(128)(2,1)}, u32[]{:S(2)}) copy-start(bf16[2048]{0:T(1024)(128)(2,1)} %param.27) | copy-start | bytes 12292
  252.4 62.9 %all-to-all-start = ((bf16[8,128,2048]{2,1,0:T(8,128)(2,1)}), bf16[8,128,2048]{2,1,0:T(8,128)(2,1)}, u32[]{:S(2)}, u32[]{:S(2)}) async-start(bf16[8,128,2048]{2,1,0:T(8,128)(2,1)} %broadcast_in_dim.7), calls=%async_computation | async-start | bytes 8388608 | tf_op jit(solution)/shard_map/all_to_all | solution.py:25
  266.4 107.3 %all-gather.10.cloned.1.call-start = ((), (), s32[]{:S(2)}) async-start(), calls=%async_computation.4 | async-start | bytes 3342336 | tf_op jit(solution)/shard_map/all_gather | solution.py:67
  310.5 7.9 %copy-start.1 = (bf16[128,2048]{1,0:T(8,128)(2,1)S(1)}, bf16[128,2048]{1,0:T(8,128)(2,1)}, u32[]{:S(2)}) copy-start(bf16[128,2048]{1,0:T(8,128)(2,1)} %param.17) | copy-start | bytes 1572868
  322.6 3.9 collective-permute-start
  325.1 4.8 %collective-permute-start.1 = (bf16[1,1408]{1,0:T(2,128)(2,1)S(1)}, bf16[1,1408]{1,0:T(2,128)(2,1)S(1)}, u32[]{:S(2)}, u32[]{:S(2)}) collective-permute-start(bf16[1,1408]{1,0:T(2,128)(2,1)S(1)} %get-tuple-element.9), channel_id=1, source_target_pairs={{8,0},{16,8},{24,16},{32,24},{40,32},{48,40},{56,48},{64,56},{72,6... | collective-permute-start | bytes 8456 | tf_op jit(solution)/shard_map/ppermute | solution.py:60
  330.0 61.7 %copy-start.6 = (bf16[2048]{0:T(1024)(128)(2,1)S(1)}, bf16[2048]{0:T(1024)(128)(2,1)}, u32[]{:S(2)}) copy-start(bf16[2048]{0:T(1024)(128)(2,1)} %param.28) | copy-start | bytes 12292
  377.6 23.4 %all-to-all-start.1 = ((bf16[8,16,2048]{2,1,0:T(8,128)(2,1)}), bf16[8,16,2048]{2,1,0:T(8,128)(2,1)S(1)}, u32[]{:S(2)}, u32[]{:S(2)}) async-start(bf16[8,16,2048]{2,1,0:T(8,128)(2,1)} %bitcast.18), calls=%async_computation.1 | async-start | bytes 1048576 | tf_op jit(solution)/shard_map/all_to_all | solution.py:79
Sparse Core Ops, SparseCore 0:
  9.4 67.2 all-gather.11
  79.6 149.0 all-gather.5
  230.9 73.7 all-gather.7
  306.6 67.1 all-gather.9
where the time goes:
time: 409 us; the launch traced here: 408 us
  waiting for transfers between devices  300 us (73%)
  starting transfers between devices  32 us (8%)
  matrix products  25.3 us (6%)
  other arithmetic  15 us (4%)
  between operations  13.3 us (3%)
  blocking collectives  12 us (3%)
  local copies, waits for them, and re-layouts  10.8 us (3%)
    all_gather x1, waiting for transfers between devices, side_by_side(): whole, at, outs = (lax.all_gather(both, axis, axis=dim, tiled=True), 0, [])  150 us
    all_gather x2, waiting for transfers between devices, stacked_from(): pieces = lax.all_gather(pieces, axes[k], axis=0, tiled=True)  89.5 us
    all_gather x1, waiting for transfers between devices, whole_of(): x = lax.all_gather(x, axis, axis=dim, tiled=True)  43.6 us
    all_to_all x1, starting transfers between devices, sent_to_all(): lax.all_to_all(jnp.broadcast_to(x[None], (size, *x.shape)), axis, 0, 0, t...  14.1 us
    all_to_all x1, starting transfers between devices, sum_at_owner(): pieces = lax.all_to_all(split_up(x, dim, size), axis, 0, 0, tiled=True)  14 us
    all_gather x1, blocking collectives, whole_of(): x = lax.all_gather(x, axis, axis=dim, tiled=True)  12 us
    all_to_all x1, waiting for transfers between devices, sum_at_owner(): pieces = lax.all_to_all(split_up(x, dim, size), axis, 0, 0, tiled=True)  9.23 us
  transfers between devices with their start and end apart: 8, of which 7 were waited for; matrix products, arithmetic and copies ran while one was open for 11% of the time, Pallas kernels for 0%

commit v1 on v0

--- a/solution.py
+++ b/solution.py
@@ -38,7 +38,8 @@
 def stacked_from(x, axes, order):
     pieces = x[None]
     for k in order:
-        pieces = lax.all_gather(pieces, axes[k], axis=0, tiled=True)
+        repeated = jnp.stack([pieces] * lax.axis_size(axes[k]))
+        pieces = jnp.concatenate(lax.all_to_all(repeated, axes[k], 0, 0), axis=0)
     current = [lax.axis_size(axes[k]) for k in reversed(order)]
     pieces = pieces.reshape(*current, *x.shape)
     turned = sorted(range(len(order)), key=lambda place: order[len(order) - 1 - place])

time: 409 us -> 364 us (0.89)
  waiting for transfers between devices: 300 us -> 169 us
  blocking collectives: 12 us -> 94.6 us
    all_gather x2 -> x0, waiting for transfers between devices: 89.5 us -> none  [stacked_from(): pieces = lax.all_gather(pieces, axes[k], axis=0, tiled=True)]
    all_to_all x0 -> x1, blocking collectives: none -> 83.7 us  [stacked_from(): pieces = jnp.concatenate(lax.all_to_all(repeated, axes[k], 0, 0), axis=0)]
    all_gather x1, waiting for transfers between devices: 150 us -> 113 us  [side_by_side(): whole, at, outs = (lax.all_gather(both, axis, axis=dim, tiled=True), 0, [])]
    all_gather x1, waiting for transfers between devices: 43.6 us -> 12.4 us  [whole_of(): x = lax.all_gather(x, axis, axis=dim, tiled=True)]
    all_to_all x1, waiting for transfers between devices: 4.73 us -> 31.1 us  [sent_to_all(): lax.all_to_all(jnp.broadcast_to(x[None], (size, *x.shape)), axis, 0, 0, t...]
    all_to_all x0 -> x1, local copies, waits for them, and re-layouts: none -> 5.89 us  [stacked_from(): pieces = jnp.concatenate(lax.all_to_all(repeated, axes[k], 0, 0), axis=0)]
    transpose x1 -> x0, local copies, waits for them, and re-layouts: 5.83 us -> none  [stacked_from(): pieces.transpose(*turned, *range(len(order), pieces.ndim))]
    all_to_all x0 -> x1, starting transfers between devices: none -> 5.28 us  [stacked_from(): pieces = jnp.concatenate(lax.all_to_all(repeated, axes[k], 0, 0), axis=0)]
  transfers between devices with their start and end apart: 8 -> 7, of which waited for: 7 -> 5; matrix products, arithmetic and copies ran while one was open for 11% -> 11% of each run, Pallas kernels for 0% -> 0%
where the time goes in v1:
time: 364 us; the launch traced here: 363 us
  waiting for transfers between devices  169 us (46%)
  blocking collectives  94.6 us (26%)
  starting transfers between devices  31.3 us (9%)
  matrix products  25.5 us (7%)
  between operations  15.1 us (4%)
  local copies, waits for them, and re-layouts  14 us (4%)
  other arithmetic  13.6 us (4%)
    all_gather x1, waiting for transfers between devices, side_by_side(): whole, at, outs = (lax.all_gather(both, axis, axis=dim, tiled=True), 0, [])  113 us
    all_to_all x1, blocking collectives, stacked_from(): pieces = jnp.concatenate(lax.all_to_all(repeated, axes[k], 0, 0), axis=0)  83.7 us
    all_to_all x1, waiting for transfers between devices, sent_to_all(): lax.all_to_all(jnp.broadcast_to(x[None], (size, *x.shape)), axis, 0, 0, t...  31.1 us
    all_to_all x1, starting transfers between devices, sum_at_owner(): pieces = lax.all_to_all(split_up(x, dim, size), axis, 0, 0, tiled=True)  13.7 us
    all_gather x1, waiting for transfers between devices, whole_of(): x = lax.all_gather(x, axis, axis=dim, tiled=True)  12.4 us
    all_gather x1, blocking collectives, whole_of(): x = lax.all_gather(x, axis, axis=dim, tiled=True)  10.9 us
    all_to_all x1, starting transfers between devices, sent_to_all(): lax.all_to_all(jnp.broadcast_to(x[None], (size, *x.shape)), axis, 0, 0, t...  9.77 us
    all_to_all x1, waiting for transfers between devices, sum_at_owner(): pieces = lax.all_to_all(split_up(x, dim, size), axis, 0, 0, tiled=True)  9.23 us
  transfers between devices with their start and end apart: 7, of which 5 were waited for; matrix products, arithmetic and copies ran while one was open for 11% of the time, Pallas kernels for 0%

profile of v1, /device:TPU:1, one launch (start us, length us, event | category | flops | bytes accessed | tf_op | source)
XLA Modules:
  0.0 363.1 jit_solution(6099380390669855750)
XLA Ops:
  8.5 1.0 fusion.37
  12.7 83.7 %all_to_all.20 = bf16[16,1,32,1408]{3,2,1,0:T(8,128)(2,1)S(1)} all-to-all(bf16[16,1,32,1408]{3,2,1,0:T(8,128)(2,1)S(1)} %stack.29), channel_id=1, replica_groups=mesh['sp_0'=16,'sp_1'=4,'tp'=8] {'sp_0'}, dimensions={0} | all-to-all | bytes 2883584 | tf_op jit(solution)/shard_map/all_to_all | solution.py:42
  96.4 3.1 stack.30
  99.5 5.3 %all-to-all-start.2 = ((bf16[4,16,32,1408]{3,2,1,0:T(8,128)(2,1)}), bf16[4,16,32,1408]{3,2,1,0:T(8,128)(2,1)}, u32[]{:S(2)}, u32[]{:S(2)}) async-start(bf16[4,16,32,1408]{3,2,1,0:T(8,128)(2,1)} %stack.30), calls=%async_computation.2 | async-start | bytes 11534336 | tf_op jit(solution)/shard_map/all_to_all | solution.py:42
  105.0 1.5 constant_dynamic-slice_fusion.2
  106.5 112.8 %all-gather.3.cloned.1.call-done = bf16[8192,320]{1,0:T(8,128)(2,1)} async-done(((bf16[128,320]{1,0:T(8,128)(2,1)}), bf16[8192,320]{1,0:T(8,128)(2,1)}) %all-gather.3.cloned.1.call-update) | async-done | bytes 5242896 | tf_op jit(solution)/shard_map/all_gather | solution.py:16
  219.3 4.3 %convolution_bitcast_fusion = f32[1,128,8192]{1,2,0:T(8,128)} fusion(bf16[128,64]{0,1:T(8,128)(2,1)S(1)} %bitcast.52, bf16[8192,320]{1,0:T(8,128)(2,1)} %all-gather.3.cloned.1.call-done), kind=kOutput, calls=%fused_computation | convolution fusion | flops 134217728 | bytes 6307840 | tf_op jit(solution)/shard_map/qhd,kd->hqk/dot_general | solution.py:154
  223.6 7.7 %fusion.67 = (f32[128]{0:T(128)S(1)}, f32[1,128,8192]{1,2,0:T(8,128)}) fusion(f32[1,128,8192]{1,2,0:T(8,128)} %convolution_bitcast_fusion, bf16[128,1,128]{2,0,1:T(8,128)(2,1)S(1)} %copy-done.3, bf16[8192,320]{1,0:T(8,128)(2,1)} %all-gather.3.cloned.1.call-done, bf16[256,1,128]{2,1,0:T(2,128)(2,1)S(1)} %get-tuple-element.19), kind=kOutput, calls=%fused_computation.104 | convolution fusion | flops 809500544 | bytes 12681728 | tf_op jit(solution)/shard_map/qhd,khd->hqk/dot_general | solution.py:153
  231.2 3.3 fusion.2
  234.5 5.7 %fusion.20 = bf16[128,128]{1,0:T(8,128)(2,1)S(1)} fusion(bf16[8192,320]{1,0:T(8,128)(2,1)} %all-gather.3.cloned.1.call-done, f32[1,128,8192]{1,2,0:T(8,128)} %get-tuple-element.15, f32[128]{0:T(128)S(1)} %broadcast_maximum_fusion, bf16[256,1,128]{2,1,0:T(2,128)(2,1)S(1)} %get-tuple-element.18, f32[128]{0:T(128)S(1)} %fusion.2), kind=kOutput, calls=%fused_computation.21 | convolution fusion | flops 808484864 | bytes 8487936 | tf_op jit(solution)/shard_map/hqk,khd->hqd/dot_general | solution.py:159
  240.6 2.5 broadcast_in_dim.5
  243.0 9.8 %all-to-all-start = ((bf16[8,128,2048]{2,1,0:T(8,128)(2,1)}), bf16[8,128,2048]{2,1,0:T(8,128)(2,1)}, u32[]{:S(2)}, u32[]{:S(2)}) async-start(bf16[8,128,2048]{2,1,0:T(8,128)(2,1)} %broadcast_in_dim.5), calls=%async_computation | async-start | bytes 8388608 | tf_op jit(solution)/shard_map/all_to_all | solution.py:25
  252.8 10.9 %all_gather.10 = bf16[704,128]{0,1:T(8,128)(2,1)} all-gather(bf16[704,32]{0,1:T(8,128)(2,1)S(1)} %copy-done.2), channel_id=1, replica_groups=mesh['sp_0'=16,'sp_1'=4,'tp'=8] {'sp_1'}, dimensions={1}, use_global_device_ids=true | all-gather | bytes 225280 | tf_op jit(solution)/shard_map/all_gather | solution.py:68
  264.6 5.9 %copy.29 = bf16[4,16,32,1408]{3,2,0,1:T(8,128)(2,1)} copy(bf16[4,16,32,1408]{3,2,1,0:T(8,128)(2,1)} %all-to-all-done.2) | data formatting | bytes 11534336 | tf_op jit(solution)/shard_map/all_to_all | solution.py:42
  270.5 31.1 %all-to-all-done = bf16[8,128,2048]{2,1,0:T(8,128)(2,1)} async-done(((bf16[8,128,2048]{2,1,0:T(8,128)(2,1)}), bf16[8,128,2048]{2,1,0:T(8,128)(2,1)}, u32[]{:S(2)}, u32[]{:S(2)}) %all-to-all-start) | async-done | bytes 4194336 | tf_op jit(solution)/shard_map/all_to_all | solution.py:25
  301.6 3.0 reduce_sum.71
  305.3 3.7 %convolution_convert_fusion.4 = bf16[128,1408]{1,0:T(8,128)(2,1)S(1)} fusion(bf16[2048,1408]{1,0:T(8,128)(2,1)} %bitcast.50, f32[2048]{0:T(1024)S(1)} %convert_element_type.128, f32[128]{0:T(128)S(1)} %add_rsqrt_fusion.1, bf16[128,2048]{1,0:T(8,128)(2,1)S(1)} %fusion.28), kind=kOutput, calls=%fused_computation.13 | convolution fusion | flops 739426304 | bytes 6660608 | tf_op jit(solution)/shard_map/dot_general | solution.py:177
  309.0 1.3 collective-permute-start
  310.3 1.3 collective-permute-start.1
  311.7 3.3 collective-permute-done.1
  315.4 12.4 %all-gather.5.cloned.1.call-done = bf16[704,2048]{0,1:T(8,128)(2,1)} async-done(((bf16[704,128]{0,1:T(8,128)(2,1)}), bf16[704,2048]{0,1:T(8,128)(2,1)}) %all-gather.5.cloned.1.call-update) | async-done | bytes 2883600 | tf_op jit(solution)/shard_map/all_gather | solution.py:68
  327.8 3.9 %convolution_convert_fusion.2 = bf16[128,2048]{1,0:T(8,128)(2,1)} fusion(bf16[704,2048]{0,1:T(8,128)(2,1)} %all-gather.5.cloned.1.call-done, f32[128,1408]{1,0:T(8,128)S(1)} %fusion.29), kind=kOutput, calls=%fused_computation.11 | convolution fusion | flops 369901568 | bytes 4194304 | tf_op jit(solution)/shard_map/dot_general | solution.py:192
  331.7 13.7 %all-to-all-start.3 = ((bf16[8,16,2048]{2,1,0:T(8,128)(2,1)}), bf16[8,16,2048]{2,1,0:T(8,128)(2,1)S(1)}, u32[]{:S(2)}, u32[]{:S(2)}) async-start(bf16[8,16,2048]{2,1,0:T(8,128)(2,1)} %bitcast.17), calls=%async_computation.3 | async-start | bytes 1048576 | tf_op jit(solution)/shard_map/all_to_all | solution.py:80
  345.5 9.2 %all-to-all-done.3 = bf16[8,16,2048]{2,1,0:T(8,128)(2,1)S(1)} async-done(((bf16[8,16,2048]{2,1,0:T(8,128)(2,1)}), bf16[8,16,2048]{2,1,0:T(8,128)(2,1)S(1)}, u32[]{:S(2)}, u32[]{:S(2)}) %all-to-all-start.3) | async-done | bytes 524320 | tf_op jit(solution)/shard_map/all_to_all | solution.py:80
  (58 shorter events, 7.8 us)
Async XLA Ops:
  7.4 232.9 %copy-start = (bf16[128,2048]{1,0:T(8,128)(2,1)S(1)}, bf16[128,2048]{1,0:T(8,128)(2,1)}, u32[]{:S(2)}) copy-start(bf16[128,2048]{1,0:T(8,128)(2,1)} %param.25) | copy-start | bytes 1572868
  7.4 211.9 %all-gather.3.cloned.1.call-start = ((), (), s32[]{:S(2)}) async-start(), calls=%async_computation.4 | async-start | bytes 6389760 | tf_op jit(solution)/shard_map/all_gather | solution.py:16
  99.5 5.3 %copy-start.4 = (bf16[128,1,64]{0,2,1:T(8,128)(2,1)S(1)}, bf16[128,1,64]{0,2,1:T(8,128)(2,1)}, u32[]{:S(2)}) copy-start(bf16[128,1,64]{0,2,1:T(8,128)(2,1)} %param.19) | copy-start | bytes 49156
  99.5 141.0 %all-to-all-start.2 = ((bf16[4,16,32,1408]{3,2,1,0:T(8,128)(2,1)}), bf16[4,16,32,1408]{3,2,1,0:T(8,128)(2,1)}, u32[]{:S(2)}, u32[]{:S(2)}) async-start(bf16[4,16,32,1408]{3,2,1,0:T(8,128)(2,1)} %stack.30), calls=%async_computation.2 | async-start | bytes 11534336 | tf_op jit(solution)/shard_map/all_to_all | solution.py:42
  105.0 118.6 %copy-start.3 = (bf16[128,1,128]{2,0,1:T(8,128)(2,1)S(1)}, bf16[128,1,128]{2,0,1:T(8,128)(2,1)}, u32[]{:S(2)}) copy-start(bf16[128,1,128]{2,0,1:T(8,128)(2,1)} %param.18) | copy-start | bytes 98308
  243.0 9.8 %copy-start.2 = (bf16[704,32]{0,1:T(8,128)(2,1)S(1)}, bf16[704,32]{0,1:T(8,128)(2,1)}, u32[]{:S(2)}) copy-start(bf16[704,32]{0,1:T(8,128)(2,1)} %param.33) | copy-start | bytes 135172
  243.0 20.7 %copy-start.5 = (bf16[2048]{0:T(1024)(128)(2,1)S(1)}, bf16[2048]{0:T(1024)(128)(2,1)}, u32[]{:S(2)}) copy-start(bf16[2048]{0:T(1024)(128)(2,1)} %param.26) | copy-start | bytes 12292
  243.0 20.7 %copy-start.6 = (bf16[2048]{0:T(1024)(128)(2,1)S(1)}, bf16[2048]{0:T(1024)(128)(2,1)}, u32[]{:S(2)}) copy-start(bf16[2048]{0:T(1024)(128)(2,1)} %param.27) | copy-start | bytes 12292
  243.0 58.5 %all-to-all-start = ((bf16[8,128,2048]{2,1,0:T(8,128)(2,1)}), bf16[8,128,2048]{2,1,0:T(8,128)(2,1)}, u32[]{:S(2)}, u32[]{:S(2)}) async-start(bf16[8,128,2048]{2,1,0:T(8,128)(2,1)} %broadcast_in_dim.5), calls=%async_computation | async-start | bytes 8388608 | tf_op jit(solution)/shard_map/all_to_all | solution.py:25
  252.8 75.0 %all-gather.5.cloned.1.call-start = ((), (), s32[]{:S(2)}) async-start(), calls=%async_computation.5 | async-start | bytes 3342336 | tf_op jit(solution)/shard_map/all_gather | solution.py:68
  270.5 34.3 %copy-start.1 = (bf16[128,2048]{1,0:T(8,128)(2,1)S(1)}, bf16[128,2048]{1,0:T(8,128)(2,1)}, u32[]{:S(2)}) copy-start(bf16[128,2048]{1,0:T(8,128)(2,1)} %param.17) | copy-start | bytes 1572868
  309.0 2.7 collective-permute-start
  310.3 4.8 %collective-permute-start.1 = (bf16[1,1408]{1,0:T(2,128)(2,1)S(1)}, bf16[1,1408]{1,0:T(2,128)(2,1)S(1)}, u32[]{:S(2)}, u32[]{:S(2)}) collective-permute-start(bf16[1,1408]{1,0:T(2,128)(2,1)S(1)} %get-tuple-element.9), channel_id=1, source_target_pairs={{8,0},{16,8},{24,16},{32,24},{40,32},{48,40},{56,48},{64,56},{72,6... | collective-permute-start | bytes 8456 | tf_op jit(solution)/shard_map/ppermute | solution.py:61
  315.2 30.2 %copy-start.7 = (bf16[2048]{0:T(1024)(128)(2,1)S(1)}, bf16[2048]{0:T(1024)(128)(2,1)}, u32[]{:S(2)}) copy-start(bf16[2048]{0:T(1024)(128)(2,1)} %param.28) | copy-start | bytes 12292
  331.7 23.0 %all-to-all-start.3 = ((bf16[8,16,2048]{2,1,0:T(8,128)(2,1)}), bf16[8,16,2048]{2,1,0:T(8,128)(2,1)S(1)}, u32[]{:S(2)}, u32[]{:S(2)}) async-start(bf16[8,16,2048]{2,1,0:T(8,128)(2,1)} %bitcast.17), calls=%async_computation.3 | async-start | bytes 1048576 | tf_op jit(solution)/shard_map/all_to_all | solution.py:80
Sparse Core Ops, SparseCore 0:
  11.8 207.3 all-gather.2
Sparse Core Ops, SparseCore 1:
  263.8 64.0 all-gather.4
